TPU v7x, 256 devices: a whole 4x4x8 slice. The times are simulated.
256 devices in a mesh: sp: 16 (over y, x), tp: 16 (over z, core).
Axes of the slice: x: 4, y: 4, z: 8, core: 2. Of those that a mesh axis runs over, the one named last changes fastest.
Arguments:
- saved_input: bfloat16 [4096, 2048], P('sp'), may hold values from -6 to 6
- cotangent: bfloat16 [4096, 2048], P('sp'), may hold values from -6 to 6
- expert_ids: int32 [4096, 2], P('sp'), may hold values from 0 to 15, all different within a row; in each aligned block of 256 rows (0 to 255, 256 to 511, ...) at most 64 rows name the same one
- route_weight: float32 [4096, 2], P('sp'), may hold values from 0.1 to 0.9
- w_gate: bfloat16 [16, 2048, 6144], P('sp', None, 'tp'), may hold values from -0.125 to 0.125
- w_up: bfloat16 [16, 2048, 6144], P('sp', None, 'tp'), may hold values from -0.125 to 0.125
- w_down: bfloat16 [16, 6144, 2048], P('sp', 'tp'), may hold values from -0.078125 to 0.078125
- w_out: bfloat16 [2048, 2048], P(None, 'tp'), may hold values from -0.125 to 0.125
- channel_gain: float32 [2048], P('tp'), may hold values from 0.1 to 1.9
- conv_taps: float32 [31, 2048], P(None, 'tp'), may hold values from -1 to 1
- glu_value: bfloat16 [2048, 4096], P('tp', 'sp'), may hold values from -6 to 6
- glu_gate: bfloat16 [2048, 4096], P('tp', 'sp'), may hold values from -8 to 8
- conv_out: bfloat16 [2048, 4096], P('tp', 'sp'), may hold values from -6 to 6
- norm_mean: float32 [4096], P('sp'), may hold values from -3 to 3
- norm_rstd: float32 [4096], P('sp'), may hold values from 0.5 to 2
Outputs:
- gate_grad: bfloat16 [16, 2048, 6144], P('sp', None, 'tp')
- up_grad: bfloat16 [16, 2048, 6144], P('sp', None, 'tp')
- down_grad: bfloat16 [16, 6144, 2048], P('sp', 'tp')
- proj_grad: float32 [2048, 2048], P('sp', 'tp')
- value_grad: bfloat16 [2048, 4096], P('tp', 'sp')
- gate_in_grad: bfloat16 [2048, 4096], P('tp', 'sp')
Inputs may be any that keep to these rules, and one draw needn't show every extreme that they name: `expert_ids`: the two experts of a position differ. In the positions of one block of 256, no expert is named more than 64 times, a bound that some block reaches.
All inputs are finite; a program needn't handle non-finite values.
Results may differ from a plain program's by a relative error of at most 0.018.
Values may be sent and summed in bfloat16 or wider, within the bound.
No kernel may reach another device: no remote copies, remote signals or barrier semaphores. Data moves between devices by JAX's collectives and lax.ppermute only.
A program may use at most 128 MiB of HBM per device.

v0:
```python
import jax
import jax.numpy as jnp
from jax import lax
from jax.sharding import PartitionSpec as P

D = 2048
C = 2048


def in_one_piece(arrays, axis, split_dim, concat_dim, along):
    ends, at = ([], 0)
    for a in arrays[:-1]:
        at += a.shape[along]
        ends.append(at)
    both = jnp.concatenate(arrays, axis=along)
    return tuple(
        jnp.split(
            lax.all_to_all(both, axis, split_axis=split_dim, concat_axis=concat_dim, tiled=True),
            ends,
            axis=along,
        )
    )


def cut_along(value, dim, devices):
    before, after = (value.shape[:dim], value.shape[dim + 1 :])
    return jnp.moveaxis(value.reshape(*before, devices, -1, *after), dim, 0)


def sent_and_summed(value, axis, dim):
    devices = lax.axis_size(axis)
    tiles = lax.all_to_all(cut_along(value, dim, devices), axis, 0, 0, tiled=True)
    return jnp.sum(tiles.astype(jnp.float32), axis=0)


def copy_for_each(value, axis):
    copies = jnp.broadcast_to(value, (lax.axis_size(axis), *value.shape))
    return lax.all_to_all(copies, axis, split_axis=0, concat_axis=0, tiled=True)


def of_everyone(value, axis):
    everything = copy_for_each(value, axis)
    return jnp.sum(everything, axis=0)


def in_one(arrays, axis):
    ravelled, at, gathered = (jnp.concatenate([a.reshape(-1) for a in arrays]), 0, [])
    subtotal = of_everyone(ravelled, axis)
    for a in arrays:
        gathered.append(subtotal[at : at + a.size].reshape(a.shape))
        at += a.size
    return tuple(gathered)


def from_behind(value, axis, by):
    devices = lax.axis_size(axis)
    pairs = [(i, i + by) for i in range(devices) if 0 <= i + by < devices]
    return lax.ppermute(value, axis, pairs)


def contract(left, right, left_dim, right_dim):
    return lax.dot_general(
        left, right, (((left_dim,), (right_dim,)), ((), ())), preferred_element_type=jnp.float32
    )


def expert_grads(rows_in, rows_cot, gate_weight, up_weight, down_weight):
    gate_pre = jnp.dot(rows_in, gate_weight, preferred_element_type=jnp.float32)
    up_pre = jnp.dot(rows_in, up_weight, preferred_element_type=jnp.float32)
    sigma = jax.nn.sigmoid(gate_pre)
    hidden = (gate_pre * sigma * up_pre).astype(jnp.bfloat16)
    hidden_cot = contract(rows_cot, down_weight, 1, 1)
    down_part = contract(hidden, rows_cot, 0, 0).astype(jnp.bfloat16)
    gate_cot = (hidden_cot * up_pre * sigma * (1.0 + gate_pre * (1.0 - sigma))).astype(jnp.bfloat16)
    up_cot = (hidden_cot * gate_pre * sigma).astype(jnp.bfloat16)
    gate_part = contract(rows_in, gate_cot, 0, 0).astype(jnp.bfloat16)
    up_part = contract(rows_in, up_cot, 0, 0).astype(jnp.bfloat16)
    input_cot = contract(gate_cot, gate_weight, 1, 1) + contract(up_cot, up_weight, 1, 1)
    return (gate_part, up_part, down_part, input_cot)


def on_device(
    saved_input,
    cotangent,
    expert_ids,
    route_weight,
    w_gate,
    w_up,
    w_down,
    w_out,
    channel_gain,
    conv_taps,
    glu_value,
    glu_gate,
    conv_out,
    norm_mean,
    norm_rstd,
):
    tokens_here = cotangent.shape[0]
    sp_count = lax.axis_size("sp")
    local_experts = w_gate.shape[0]
    expert_count = local_experts * sp_count
    capacity = 4 * tokens_here // expert_count
    pairs = expert_ids.reshape(2 * tokens_here)
    onehot = (pairs[:, None] == jnp.arange(expert_count, dtype=jnp.int32)[None, :]).astype(
        jnp.int32
    )
    before = jnp.cumsum(onehot, axis=0) - onehot
    target = pairs * capacity + jnp.sum(before * onehot, axis=1)
    owner = (
        jnp.zeros((expert_count * capacity,), jnp.int32)
        .at[target]
        .set(jnp.arange(2 * tokens_here, dtype=jnp.int32) + 1)
    )
    filled = (owner > 0)[:, None]
    pair_index = jnp.maximum(owner - 1, 0)
    scaled = (route_weight[:, :, None] * cotangent.astype(jnp.float32)[:, None, :]).astype(
        jnp.bfloat16
    )
    scaled = scaled.reshape(2 * tokens_here, D)
    send_cot = jnp.where(filled, scaled[pair_index], jnp.zeros_like(scaled[:1])).reshape(
        expert_count, capacity, D
    )
    send_in = jnp.where(filled, saved_input[pair_index // 2], jnp.zeros_like(saved_input[:1]))
    send_in = send_in.reshape(expert_count, capacity, D)
    rows_cot, rows_in = in_one_piece((send_cot, send_in), "sp", 0, 1, 2)
    results = [expert_grads(rows_in[0], rows_cot[0], w_gate[0], w_up[0], w_down[0])]
    gate_grad = jnp.stack([result[0] for result in results])
    up_grad = jnp.stack([result[1] for result in results])
    down_grad = jnp.stack([result[2] for result in results])
    input_cot = jnp.stack([result[3] for result in results])
    blocks = input_cot.reshape(local_experts, sp_count, capacity, D)
    share = lax.psum_scatter(
        blocks.astype(jnp.bfloat16), "tp", scatter_dimension=2, tiled=True
    ).astype(jnp.float32)
    returned = lax.all_to_all(
        share.astype(jnp.bfloat16), "sp", split_axis=1, concat_axis=0, tiled=True
    ).astype(share.dtype)
    whole = lax.all_gather(returned.astype(jnp.bfloat16), "tp", axis=2, tiled=True).astype(
        returned.dtype
    )
    routed = whole.reshape(expert_count * capacity, D)[target].reshape(tokens_here, 2, D)
    summed = jnp.sum(routed, axis=1)
    mixed_cot = (cotangent.astype(jnp.float32) + summed).astype(jnp.bfloat16)
    centered = (conv_out.astype(jnp.float32) - norm_mean[None, :]) * norm_rstd[None, :]
    normed = centered * channel_gain[:, None]
    sigma = jax.nn.sigmoid(normed)
    output_act = (normed * sigma).astype(jnp.bfloat16)
    proj_grad = sent_and_summed(contract(mixed_cot, output_act, 0, 1).astype(jnp.bfloat16), "sp", 0)
    act_cot = contract(w_out, mixed_cot, 0, 1)
    norm_cot = act_cot * sigma * (1.0 + normed * (1.0 - sigma)) * channel_gain[:, None]
    first_sum, second_sum = in_one(
        (jnp.sum(norm_cot, axis=0), jnp.sum(norm_cot * centered, axis=0)), "tp"
    )
    conv_cot = norm_rstd[None, :] * (
        norm_cot - first_sum[None, :] / C - centered * second_sum[None, :] / C
    )
    reach = conv_taps.shape[0] - 1
    rim = from_behind(conv_cot[:, :reach], "sp", -1)
    padded = jnp.concatenate([conv_cot, rim], axis=1)
    glu_cot = conv_taps[0][:, None] * padded[:, :tokens_here]
    for lag in range(1, reach + 1):
        glu_cot = glu_cot + conv_taps[lag][:, None] * padded[:, lag : lag + tokens_here]
    gate_sigma = jax.nn.sigmoid(glu_gate.astype(jnp.float32))
    value_grad = (glu_cot * gate_sigma).astype(jnp.bfloat16)
    gate_in_grad = (
        glu_cot * glu_value.astype(jnp.float32) * gate_sigma * (1.0 - gate_sigma)
    ).astype(jnp.bfloat16)
    return (gate_grad, up_grad, down_grad, proj_grad, value_grad, gate_in_grad)


def solution(mesh):
    in_specs = (
        P("sp", None),
        P("sp", None),
        P("sp", None),
        P("sp", None),
        P("sp", None, "tp"),
        P("sp", None, "tp"),
        P("sp", "tp", None),
        P(None, "tp"),
        P("tp"),
        P(None, "tp"),
        P("tp", "sp"),
        P("tp", "sp"),
        P("tp", "sp"),
        P("sp"),
        P("sp"),
    )
    out_specs = (
        P("sp", None, "tp"),
        P("sp", None, "tp"),
        P("sp", "tp", None),
        P("sp", "tp"),
        P("tp", "sp"),
        P("tp", "sp"),
    )
    return jax.shard_map(
        on_device, mesh=mesh, in_specs=in_specs, out_specs=out_specs, check_vma=False
    )
```

profile of v0, /device:TPU:24, one launch (start us, length us, event | category | flops | bytes accessed | tf_op | source)
XLA Modules:
  0.0 370.5 jit_solution(13635867785435302561)
XLA Ops:
  7.2 0.0 copy-start
  7.2 0.0 reduce-scatter.2.cloned.1.call-start
  7.2 0.8 broadcast_multiply_fusion
  8.0 0.8 copy.65
  8.8 0.1 eq.25
  9.0 0.1 eq.29
  9.1 0.1 copy.64
  9.3 0.1 mul.436
  9.4 1.2 reduce-window.6
  10.6 0.2 slice_reduce_fusion
  10.9 0.1 fusion.114
  11.0 2.4 scatter_custom_fusion
  13.5 5.3 %mul.440 = f32[256,2,2048]{2,1,0:T(2,128)} broadcast(bf16[256,2048]{1,0:T(8,128)(2,1)} %param.16), dimensions={0,2} | broadcast | bytes 5242880 | tf_op jit(solution)/shard_map/mul | solution.py:117
  18.8 6.1 %mul.441 = f32[512,2048]{1,0:T(8,128)} reshape(f32[256,2,2048]{2,1,0:T(2,128)} %mul.440) | data formatting | bytes 8388608 | tf_op jit(solution)/shard_map/mul | solution.py:117
  24.9 0.1 copy.68
  25.0 0.1 mul.438
  25.2 0.1 broadcast_in_dim.46
  25.2 3.8 %multiply_convert_fusion = bf16[512,2048]{1,0:T(8,128)(2,1)} fusion(f32[512,2048]{1,0:T(8,128)} %mul.441, f32[512]{0:T(512)S(1)} %mul.438), kind=kLoop, calls=%fused_computation.8 | loop fusion | flops 2097152 | bytes 6293504 | tf_op jit(solution)/shard_map/convert_element_type | solution.py:117
  29.0 10.8 %gather_fusion = bf16[1024,2048]{1,0:T(8,128)(2,1)} fusion(bf16[512,2048]{1,0:T(8,128)(2,1)} %multiply_convert_fusion, s32[1024]{0:T(1024)S(1)} %get-tuple-element.73), kind=kCustom, calls=%fused_computation | custom fusion | bytes 8392704 | tf_op jit(solution)/shard_map/gather | solution.py:121
  39.8 6.0 %gather_fusion.1 = bf16[1024,2048]{1,0:T(8,128)(2,1)} fusion(bf16[256,2048]{1,0:T(8,128)(2,1)S(1)} %copy-done.2, s32[1024]{0:T(1024)S(1)} %get-tuple-element.74), kind=kCustom, calls=%fused_computation.1 | custom fusion | bytes 8392704 | tf_op jit(solution)/shard_map/gather | solution.py:124
  45.8 5.8 %broadcast_select_fusion.1 = (bf16[16,64,2048]{2,1,0:T(8,128)(2,1)}, bf16[16,64,2048]{2,1,0:T(8,128)(2,1)}) fusion(bf16[16,64,2048]{2,1,0:T(8,128)(2,1)} %bitcast.144, pred[16,64]{1,0:T(8,128)(4,1)S(1)} %broadcast_in_dim.46, bf16[16,64,2048]{2,1,0:T(8,128)(2,1)} %bitcast.145), kind=kLoop, calls=%fused_computation.10 | loop fusion | flops 4194304 | bytes 16778240 | tf_op jit(solution)/shard_map/jit(_where)/select_n | solution.py:121
  51.6 7.8 %pad_maximum_fusion = bf16[16,64,4096]{2,1,0:T(8,128)(2,1)} fusion(bf16[16,64,2048]{2,1,0:T(8,128)(2,1)} %get-tuple-element.78, bf16[16,64,2048]{2,1,0:T(8,128)(2,1)} %get-tuple-element.77), kind=kLoop, calls=%fused_computation.4 | loop fusion | flops 16777216 | bytes 16777216 | tf_op jit(solution)/shard_map/concatenate | solution.py:15
  59.4 101.1 %all_to_all.35 = bf16[16,64,4096]{2,1,0:T(8,128)(2,1)S(1)} all-to-all(bf16[16,64,4096]{2,1,0:T(8,128)(2,1)} %pad_maximum_fusion), channel_id=1, replica_groups=mesh['sp'=16,'tp'=16] {'sp'}, dimensions={0} | all-to-all | bytes 16777216 | tf_op jit(solution)/shard_map/all_to_all | solution.py:18
  160.6 2.3 fusion.3
  162.9 0.2 copy-done.5
  163.1 2.3 fusion.4
  165.5 0.2 copy-done.15
  165.7 2.8 multiply_convert_fusion.2
  168.5 2.4 fusion.8
  170.9 2.4 add_convert_fusion
  173.3 4.3 %copy.69 = bf16[1,16,64,2048]{3,1,0,2:T(8,128)(2,1)} copy(bf16[1,16,64,2048]{3,2,1,0:T(8,128)(2,1)S(1)} %bitcast.146) | data formatting | bytes 8388608 | tf_op jit(solution)/shard_map/convert_element_type | solution.py:134
  177.6 0.0 reduce-scatter.2.cloned.1.call-update
  177.6 0.0 all-gather.3.cloned.1.call-start
  177.6 64.5 %reduce-scatter.2.cloned.1.call-done = bf16[1,16,4,2048]{3,1,0,2:T(8,128)(2,1)} async-done(((bf16[1,16,64,2048]{3,1,0,2:T(8,128)(2,1)}), bf16[1,16,4,2048]{3,1,0,2:T(8,128)(2,1)}) %reduce-scatter.2.cloned.1.call-update) | async-done | bytes 262160 | tf_op jit(solution)/shard_map/reduce_scatter | solution.py:133
  242.2 1.2 copy.70
  243.3 13.6 %all_to_all.36 = bf16[1,16,4,2048]{3,2,0,1:T(4,128)(2,1)S(1)} all-to-all(bf16[1,16,4,2048]{3,2,0,1:T(4,128)(2,1)S(1)} %copy.70), channel_id=1, replica_groups=mesh['sp'=16,'tp'=16] {'sp'}, dimensions={1} | all-to-all | bytes 524288 | tf_op jit(solution)/shard_map/all_to_all | solution.py:136
  256.9 0.9 copy.71
  257.8 0.0 all-gather.3.cloned.1.call-update
  257.8 0.1 copy.73
  257.9 0.1 copy.76
  258.1 0.1 copy.75
  258.3 0.0 copy-start.19
  258.3 5.9 %fusion.5 = bf16[1,2048,384]{2,1,0:T(8,128)(2,1)} fusion(bf16[1024,384]{1,0:T(8,128)(2,1)S(1)} %get-tuple-element.41, bf16[1,1024,4096]{2,1,0:T(8,128)(2,1)} %bitcast.150), kind=kOutput, calls=%fused_computation.18 | convolution fusion | flops 1611399168 | bytes 6553600 | tf_op jit(solution)/shard_map/dot_general | solution.py:62
  264.1 5.4 %fusion.7 = bf16[1,384,2048]{2,1,0:T(8,128)(2,1)} fusion(bf16[1,1024,4096]{2,1,0:T(8,128)(2,1)} %bitcast.151, f32[1024,384]{1,0:T(8,128)S(1)} %copy-done.19, f32[1024,384]{1,0:T(8,128)S(1)} %copy-done.17), kind=kOutput, calls=%fused_computation.20 | convolution fusion | flops 1613758464 | bytes 8912896 | tf_op jit(solution)/shard_map/dot_general | solution.py:62
  269.5 26.8 %all-gather.3.cloned.1.call-done = bf16[1,16,64,2048]{3,1,0,2:T(8,128)(2,1)} async-done(((bf16[1,16,4,2048]{3,1,0,2:T(8,128)(2,1)}), bf16[1,16,64,2048]{3,1,0,2:T(8,128)(2,1)}) %all-gather.3.cloned.1.call-update) | async-done | bytes 4194320 | tf_op jit(solution)/shard_map/all_gather | solution.py:139
  296.3 7.8 %copy.72 = f32[1,16,64,2048]{3,2,1,0:T(8,128)} copy(bf16[1,16,64,2048]{3,1,0,2:T(8,128)(2,1)} %all-gather.3.cloned.1.call-done) | data formatting | bytes 12582912 | tf_op jit(solution)/shard_map/reshape | solution.py:142
  304.2 8.8 %gather_fusion.2 = f32[512,2048]{1,0:T(8,128)} fusion(f32[1024,2048]{1,0:T(8,128)} %bitcast.143, s32[1024]{0:T(1024)S(1)} %pad_clamp_fusion), kind=kCustom, calls=%fused_computation.2 | custom fusion | bytes 8390656 | tf_op jit(solution)/shard_map/gather | solution.py:142
  312.9 6.0 %reshape.159 = f32[256,2,2048]{2,1,0:T(2,128)} reshape(f32[512,2048]{1,0:T(8,128)} %gather_fusion.2) | data formatting | bytes 8388608 | tf_op jit(solution)/shard_map/reshape | solution.py:142
  319.0 0.0 copy-start.3
  319.0 0.0 copy-start.6
  319.0 8.6 %reduce_sum.58 = f32[256,2048]{1,0:T(8,128)} reduce(f32[256,2,2048]{2,1,0:T(2,128)} %reshape.159, f32[]{:T(128)} %constant.44.clone.1), dimensions={1}, to_apply=%region_5.6 | reduce | flops 524288 | bytes 6291460 | tf_op jit(solution)/shard_map/reduce_sum | solution.py:143
  327.7 2.1 fusion.123
  329.8 0.6 broadcast_in_dim.51
  330.5 4.4 %all-to-all-start.3 = ((f32[16,1,512]{2,1,0:T(1,128)}), f32[16,1,512]{2,1,0:T(1,128)S(1)}, u32[]{:S(2)}, u32[]{:S(2)}) async-start(f32[16,1,512]{2,1,0:T(1,128)} %broadcast_in_dim.51), calls=%async_computation.4 | async-start | bytes 65536 | tf_op jit(solution)/shard_map/all_to_all | solution.py:38
  334.9 3.1 convolution_convert_fusion.2
  337.9 4.6 %all-to-all-done.3 = f32[16,1,512]{2,1,0:T(1,128)S(1)} async-done(((f32[16,1,512]{2,1,0:T(1,128)}), f32[16,1,512]{2,1,0:T(1,128)S(1)}, u32[]{:S(2)}, u32[]{:S(2)}) %all-to-all-start.3) | async-done | bytes 32800 | tf_op jit(solution)/shard_map/all_to_all | solution.py:38
  342.5 7.2 %all-to-all-start.2 = ((bf16[16,128,128]{2,1,0:T(8,128)(2,1)}), bf16[16,128,128]{2,1,0:T(8,128)(2,1)S(1)}, u32[]{:S(2)}, u32[]{:S(2)}) async-start(bf16[16,128,128]{2,1,0:T(8,128)(2,1)} %bitcast.16), calls=%async_computation.3 | async-start | bytes 1048576 | tf_op jit(solution)/shard_map/all_to_all | solution.py:32
  349.8 0.2 subtract_multiply_fusion
  350.0 4.9 %collective-permute-start = (f32[128,30]{0,1:T(8,128)S(1)}, f32[128,30]{0,1:T(8,128)S(1)}, u32[]{:S(2)}, u32[]{:S(2)}) collective-permute-start(f32[128,30]{0,1:T(8,128)S(1)} %slice.271), channel_id=1, source_target_pairs={{16,0},{32,16},{48,32},{64,48},{80,64},{96,80},{112,96},{128,112},... | collective-permute-start | bytes 46088 | tf_op jit(solution)/shard_map/ppermute | solution.py:58
  354.9 5.8 %fusion.6 = bf16[1,2048,384]{2,1,0:T(8,128)(2,1)} fusion(bf16[1024,384]{1,0:T(8,128)(2,1)S(1)} %get-tuple-element.40, bf16[1,1024,4096]{2,1,0:T(8,128)(2,1)} %bitcast.152), kind=kOutput, calls=%fused_computation.19 | convolution fusion | flops 1611399168 | bytes 6553600 | tf_op jit(solution)/shard_map/dot_general | solution.py:62
  360.8 0.4 multiply_convert_fusion.5
  361.2 0.7 copy.77
  362.0 0.7 copy.78
  362.7 0.7 convert_reduce_fusion
  (51 shorter events, 0.3 us)
Async XLA Ops:
  7.2 153.4 %copy-start = (bf16[1,2048,384]{2,1,0:T(8,128)(2,1)S(1)}, bf16[1,2048,384]{2,1,0:T(8,128)(2,1)}, u32[]{:S(2)}) copy-start(bf16[1,2048,384]{2,1,0:T(8,128)(2,1)} %param.19) | copy-start | bytes 4718596
  7.2 235.0 %reduce-scatter.2.cloned.1.call-start = ((), (), s32[]{:S(2)}) async-start(), calls=%async_computation.5 | async-start | bytes 4456448 | tf_op jit(solution)/shard_map/reduce_scatter | solution.py:133
  18.8 6.1 %copy-start.13 = (f32[256,2]{0,1:T(2,128)S(1)}, f32[256,2]{0,1:T(2,128)}, u32[]{:S(2)}) copy-start(f32[256,2]{0,1:T(2,128)} %param.18) | copy-start | bytes 6148
  29.0 10.8 %copy-start.2 = (bf16[256,2048]{1,0:T(8,128)(2,1)S(1)}, bf16[256,2048]{1,0:T(8,128)(2,1)}, u32[]{:S(2)}) copy-start(bf16[256,2048]{1,0:T(8,128)(2,1)} %param.15) | copy-start | bytes 3145732
  160.6 4.9 %copy-start.4 = (bf16[16,64,4096]{2,1,0:T(8,128)(2,1)}, bf16[16,64,4096]{2,1,0:T(8,128)(2,1)S(1)}, u32[]{:S(2)}) copy-start(bf16[16,64,4096]{2,1,0:T(8,128)(2,1)S(1)} %all_to_all.35) | copy-start | bytes 25165828
  160.6 2.6 copy-start.5
  163.1 2.4 copy-start.16
  163.1 2.6 copy-start.15
  165.7 2.8 copy-start.18
  177.6 80.2 %copy-start.7 = (bf16[128,256]{1,0:T(8,128)(2,1)S(1)}, bf16[128,256]{1,0:T(8,128)(2,1)}, u32[]{:S(2)}) copy-start(bf16[128,256]{1,0:T(8,128)(2,1)} %param.27) | copy-start | bytes 196612
  177.6 80.4 %copy-start.8 = (bf16[128,256]{1,0:T(8,128)(2,1)S(1)}, bf16[128,256]{1,0:T(8,128)(2,1)}, u32[]{:S(2)}) copy-start(bf16[128,256]{1,0:T(8,128)(2,1)} %param.25) | copy-start | bytes 196612
  177.6 80.5 %copy-start.9 = (bf16[128,256]{1,0:T(8,128)(2,1)S(1)}, bf16[128,256]{1,0:T(8,128)(2,1)}, u32[]{:S(2)}) copy-start(bf16[128,256]{1,0:T(8,128)(2,1)} %param.26) | copy-start | bytes 196612
  177.6 80.6 %copy-start.10 = (f32[31,128]{1,0:T(8,128)S(1)}, f32[31,128]{1,0:T(8,128)}, u32[]{:S(2)}) copy-start(f32[31,128]{1,0:T(8,128)} %param.24) | copy-start | bytes 47620
  177.6 118.7 %all-gather.3.cloned.1.call-start = ((), (), s32[]{:S(2)}) async-start(), calls=%async_computation.6 | async-start | bytes 4456448 | tf_op jit(solution)/shard_map/all_gather | solution.py:139
  258.2 5.9 %copy-start.17 = (f32[1024,384]{1,0:T(8,128)S(1)}, f32[1024,384]{1,0:T(8,128)}, u32[]{:S(2)}) copy-start(f32[1024,384]{1,0:T(8,128)} %copy-done.16) | copy-start | bytes 4718596
  258.3 5.9 %copy-start.19 = (f32[1024,384]{1,0:T(8,128)S(1)}, f32[1024,384]{1,0:T(8,128)}, u32[]{:S(2)}) copy-start(f32[1024,384]{1,0:T(8,128)} %copy-done.18) | copy-start | bytes 4718596
  319.0 8.7 %copy-start.3 = (bf16[256,2048]{1,0:T(8,128)(2,1)S(1)}, bf16[256,2048]{1,0:T(8,128)(2,1)}, u32[]{:S(2)}) copy-start(bf16[256,2048]{1,0:T(8,128)(2,1)} %param.16) | copy-start | bytes 3145732
  319.0 8.7 %copy-start.6 = (bf16[2048,128]{1,0:T(8,128)(2,1)S(1)}, bf16[2048,128]{1,0:T(8,128)(2,1)}, u32[]{:S(2)}) copy-start(bf16[2048,128]{1,0:T(8,128)(2,1)} %param.22) | copy-start | bytes 1572868
  319.0 8.7 %copy-start.11 = (f32[256]{0:T(256)S(1)}, f32[256]{0:T(256)}, u32[]{:S(2)}) copy-start(f32[256]{0:T(256)} %param.29) | copy-start | bytes 3076
  319.0 8.7 %copy-start.12 = (f32[256]{0:T(256)S(1)}, f32[256]{0:T(256)}, u32[]{:S(2)}) copy-start(f32[256]{0:T(256)} %param.28) | copy-start | bytes 3076
  319.0 8.7 %copy-start.14 = (f32[128]{0:T(128)S(1)}, f32[128]{0:T(128)}, u32[]{:S(2)}) copy-start(f32[128]{0:T(128)} %param.23) | copy-start | bytes 1540
  330.5 12.1 %all-to-all-start.3 = ((f32[16,1,512]{2,1,0:T(1,128)}), f32[16,1,512]{2,1,0:T(1,128)S(1)}, u32[]{:S(2)}, u32[]{:S(2)}) async-start(f32[16,1,512]{2,1,0:T(1,128)} %broadcast_in_dim.51), calls=%async_computation.4 | async-start | bytes 65536 | tf_op jit(solution)/shard_map/all_to_all | solution.py:38
  342.5 20.2 %all-to-all-start.2 = ((bf16[16,128,128]{2,1,0:T(8,128)(2,1)}), bf16[16,128,128]{2,1,0:T(8,128)(2,1)S(1)}, u32[]{:S(2)}, u32[]{:S(2)}) async-start(bf16[16,128,128]{2,1,0:T(8,128)(2,1)} %bitcast.16), calls=%async_computation.3 | async-start | bytes 1048576 | tf_op jit(solution)/shard_map/all_to_all | solution.py:32
  350.0 10.7 %collective-permute-start = (f32[128,30]{0,1:T(8,128)S(1)}, f32[128,30]{0,1:T(8,128)S(1)}, u32[]{:S(2)}, u32[]{:S(2)}) collective-permute-start(f32[128,30]{0,1:T(8,128)S(1)} %slice.271), channel_id=1, source_target_pairs={{16,0},{32,16},{48,32},{64,48},{80,64},{96,80},{112,96},{128,112},... | collective-permute-start | bytes 46088 | tf_op jit(solution)/shard_map/ppermute | solution.py:58
  354.9 8.5 %copy-start.1 = (bf16[1,2048,384]{2,1,0:T(8,128)(2,1)S(1)}, bf16[1,2048,384]{2,1,0:T(8,128)(2,1)}, u32[]{:S(2)}) copy-start(bf16[1,2048,384]{2,1,0:T(8,128)(2,1)} %param.19) | copy-start | bytes 4718596
Sparse Core Ops, SparseCore 0:
  177.7 64.3 reduce-scatter.1
  257.9 38.3 all-gather.2
where the time goes:
time: 377 us; the launch traced here: 370 us
  blocking collectives  115 us (31%)
  waiting for transfers between devices  95.9 us (25%)
  local copies, waits for them, and re-layouts  64.5 us (17%)
  matrix products  34.5 us (9%)
  other arithmetic  29.5 us (8%)
  starting transfers between devices  16.6 us (4%)
  between operations  14.6 us (4%)
    all_to_all x1, blocking collectives, in_one_piece(): lax.all_to_all(both, axis, split_axis=split_dim, concat_axis=concat_dim,...  101 us
    reduce_scatter x1, waiting for transfers between devices, on_device(): lax.psum_scatter(blocks.astype(jnp.bfloat16), 'tp', scatter_dimension=2,...  64.5 us
    dot_general x8, matrix products, contract(): lax.dot_general(left, right, (((left_dim,), (right_dim,)), ((), ())), pre...  29.9 us
    all_gather x1, waiting for transfers between devices, on_device(): lax.all_gather(returned.astype(jnp.bfloat16), 'tp', axis=2, tiled=True)  26.8 us
    reshape x2, local copies, waits for them, and re-layouts, on_device(): whole.reshape(expert_count * capacity, D)[target].reshape(tokens_here, 2, D)  13.9 us
    all_to_all x1, blocking collectives, on_device(): lax.all_to_all(share.astype(jnp.bfloat16), 'sp', split_axis=1, concat_axi...  13.6 us
    mul x3, local copies, waits for them, and re-layouts, on_device(): route_weight[:, :, None] * cotangent.astype(jnp.float32)[:, None, :]  11.6 us
    gather x1, local copies, waits for them, and re-layouts, on_device(): scaled[pair_index]  10.8 us
  transfers between devices with their start and end apart: 5, of which 3 were waited for; matrix products, arithmetic and copies ran while one was open for 6% of the time, Pallas kernels for 0%

commit v1 on v0

--- a/solution.py
+++ b/solution.py
@@ -1,3 +1,4 @@
+import functools
 import jax
 import jax.numpy as jnp
 from jax import lax
@@ -5,6 +6,14 @@
 
 D = 2048
 C = 2048
+
+
+def use_forms(mat, k_dim):
+    h_now = jnp.concatenate(lax.all_gather(mat, "tp"), axis=k_dim)
+    return h_now
+
+
+draft_edge_over_axis = functools.partial(use_forms, k_dim=2)
 
 
 def in_one_piece(arrays, axis, split_dim, concat_dim, along):
@@ -136,9 +145,7 @@
     returned = lax.all_to_all(
         share.astype(jnp.bfloat16), "sp", split_axis=1, concat_axis=0, tiled=True
     ).astype(share.dtype)
-    whole = lax.all_gather(returned.astype(jnp.bfloat16), "tp", axis=2, tiled=True).astype(
-        returned.dtype
-    )
+    whole = draft_edge_over_axis(returned.astype(jnp.bfloat16)).astype(returned.dtype)
     routed = whole.reshape(expert_count * capacity, D)[target].reshape(tokens_here, 2, D)
     summed = jnp.sum(routed, axis=1)
     mixed_cot = (cotangent.astype(jnp.float32) + summed).astype(jnp.bfloat16)

time: 377 us -> 398 us (1.056)
  local copies, waits for them, and re-layouts: 64.5 us -> 78.7 us
  other arithmetic: 29.5 us -> 36 us
    convert_element_type x0 -> x2, local copies, waits for them, and re-layouts: none -> 22 us  [on_device(): draft_edge_over_axis(returned.astype(jnp.bfloat16)).astype(returned.dtype)]
    reshape x2 -> x1, local copies, waits for them, and re-layouts: 13.9 us -> 5.84 us  [on_device(): whole.reshape(expert_count * capacity, D)[target].reshape(tokens_here, 2, D)]
    convert_element_type x0 -> x1, other arithmetic: none -> 6.48 us  [on_device(): draft_edge_over_axis(returned.astype(jnp.bfloat16)).astype(returned.dtype)]
where the time goes in v1:
time: 398 us; the launch traced here: 391 us
  blocking collectives  115 us (29%)
  waiting for transfers between devices  95.9 us (24%)
  local copies, waits for them, and re-layouts  78.7 us (20%)
  other arithmetic  36 us (9%)
  matrix products  34.6 us (9%)
  starting transfers between devices  16.8 us (4%)
  between operations  14.7 us (4%)
    all_to_all x1, blocking collectives, in_one_piece(): lax.all_to_all(both, axis, split_axis=split_dim, concat_axis=concat_dim,...  101 us
    reduce_scatter x1, waiting for transfers between devices, on_device(): lax.psum_scatter(blocks.astype(jnp.bfloat16), 'tp', scatter_dimension=2,...  64.5 us
    dot_general x8, matrix products, contract(): lax.dot_general(left, right, (((left_dim,), (right_dim,)), ((), ())), pre...  29.9 us
    all_gather x1, waiting for transfers between devices, use_forms(): h_now = jnp.concatenate(lax.all_gather(mat, 'tp'), axis=k_dim)  26.8 us
    convert_element_type x2, local copies, waits for them, and re-layouts, on_device(): draft_edge_over_axis(returned.astype(jnp.bfloat16)).astype(returned.dtype)  22 us
    all_to_all x1, blocking collectives, on_device(): lax.all_to_all(share.astype(jnp.bfloat16), 'sp', split_axis=1, concat_axi...  13.6 us
    mul x3, local copies, waits for them, and re-layouts, on_device(): route_weight[:, :, None] * cotangent.astype(jnp.float32)[:, None, :]  11.6 us
    gather x1, local copies, waits for them, and re-layouts, on_device(): scaled[pair_index]  10.8 us
  transfers between devices with their start and end apart: 5, of which 3 were waited for; matrix products, arithmetic and copies ran while one was open for 6% of the time, Pallas kernels for 0%

profile of v1, /device:TPU:24, one launch (start us, length us, event | category | flops | bytes accessed | tf_op | source)
XLA Modules:
  0.0 391.4 jit_solution(15545123315410769565)
XLA Ops:
  7.2 0.0 copy-start
  7.2 0.0 reduce-scatter.2.cloned.1.call-start
  7.2 0.8 broadcast_multiply_fusion
  8.0 0.8 copy.67
  8.8 0.1 eq.25
  9.0 0.1 eq.29
  9.1 0.1 copy.66
  9.3 0.1 mul.436
  9.4 1.2 reduce-window.6
  10.6 0.2 slice_reduce_fusion
  10.9 0.1 fusion.114
  11.0 2.4 scatter_custom_fusion
  13.5 5.3 %mul.440 = f32[256,2,2048]{2,1,0:T(2,128)} broadcast(bf16[256,2048]{1,0:T(8,128)(2,1)} %param.16), dimensions={0,2} | broadcast | bytes 5242880 | tf_op jit(solution)/shard_map/mul | solution.py:126
  18.8 6.1 %mul.441 = f32[512,2048]{1,0:T(8,128)} reshape(f32[256,2,2048]{2,1,0:T(2,128)} %mul.440) | data formatting | bytes 8388608 | tf_op jit(solution)/shard_map/mul | solution.py:126
  24.9 0.1 copy.70
  25.0 0.1 mul.438
  25.2 0.1 broadcast_in_dim.46
  25.2 3.8 multiply_convert_fusion
  29.0 10.8 %gather_fusion = bf16[1024,2048]{1,0:T(8,128)(2,1)} fusion(bf16[512,2048]{1,0:T(8,128)(2,1)} %multiply_convert_fusion, s32[1024]{0:T(1024)S(1)} %get-tuple-element.73), kind=kCustom, calls=%fused_computation | custom fusion | bytes 8392704 | tf_op jit(solution)/shard_map/gather | solution.py:130
  39.8 6.0 %gather_fusion.1 = bf16[1024,2048]{1,0:T(8,128)(2,1)} fusion(bf16[256,2048]{1,0:T(8,128)(2,1)S(1)} %copy-done.2, s32[1024]{0:T(1024)S(1)} %get-tuple-element.74), kind=kCustom, calls=%fused_computation.1 | custom fusion | bytes 8392704 | tf_op jit(solution)/shard_map/gather | solution.py:133
  45.8 5.8 %broadcast_select_fusion.1 = (bf16[16,64,2048]{2,1,0:T(8,128)(2,1)}, bf16[16,64,2048]{2,1,0:T(8,128)(2,1)}) fusion(bf16[16,64,2048]{2,1,0:T(8,128)(2,1)} %bitcast.149, pred[16,64]{1,0:T(8,128)(4,1)S(1)} %broadcast_in_dim.46, bf16[16,64,2048]{2,1,0:T(8,128)(2,1)} %bitcast.150), kind=kLoop, calls=%fused_computation.11 | loop fusion | flops 4194304 | bytes 16778240 | tf_op jit(solution)/shard_map/jit(_where)/select_n | solution.py:130
  51.6 7.8 %pad_maximum_fusion = bf16[16,64,4096]{2,1,0:T(8,128)(2,1)} fusion(bf16[16,64,2048]{2,1,0:T(8,128)(2,1)} %get-tuple-element.78, bf16[16,64,2048]{2,1,0:T(8,128)(2,1)} %get-tuple-element.77), kind=kLoop, calls=%fused_computation.4 | loop fusion | flops 16777216 | bytes 16777216 | tf_op jit(solution)/shard_map/concatenate | solution.py:24
  59.4 101.2 %all_to_all.35 = bf16[16,64,4096]{2,1,0:T(8,128)(2,1)S(1)} all-to-all(bf16[16,64,4096]{2,1,0:T(8,128)(2,1)} %pad_maximum_fusion), channel_id=1, replica_groups=mesh['sp'=16,'tp'=16] {'sp'}, dimensions={0} | all-to-all | bytes 16777216 | tf_op jit(solution)/shard_map/all_to_all | solution.py:27
  160.6 2.3 fusion.3
  163.0 0.2 copy-done.5
  163.2 2.3 fusion.4
  165.6 0.2 copy-done.15
  165.8 2.8 multiply_convert_fusion.2
  168.6 2.4 fusion.8
  170.9 2.4 add_convert_fusion
  173.4 4.3 %copy.71 = bf16[1,16,64,2048]{3,1,0,2:T(8,128)(2,1)} copy(bf16[1,16,64,2048]{3,2,1,0:T(8,128)(2,1)S(1)} %bitcast.151) | data formatting | bytes 8388608 | tf_op jit(solution)/shard_map/convert_element_type | solution.py:143
  177.6 0.0 reduce-scatter.2.cloned.1.call-update
  177.7 0.0 all-gather.3.cloned.1.call-start
  177.7 64.5 %reduce-scatter.2.cloned.1.call-done = bf16[1,16,4,2048]{3,1,0,2:T(8,128)(2,1)} async-done(((bf16[1,16,64,2048]{3,1,0,2:T(8,128)(2,1)}), bf16[1,16,4,2048]{3,1,0,2:T(8,128)(2,1)}) %reduce-scatter.2.cloned.1.call-update) | async-done | bytes 262160 | tf_op jit(solution)/shard_map/reduce_scatter | solution.py:142
  242.2 1.2 copy.72
  243.4 13.6 %all_to_all.36 = bf16[1,16,4,2048]{3,2,0,1:T(4,128)(2,1)S(1)} all-to-all(bf16[1,16,4,2048]{3,2,0,1:T(4,128)(2,1)S(1)} %copy.72), channel_id=1, replica_groups=mesh['sp'=16,'tp'=16] {'sp'}, dimensions={1} | all-to-all | bytes 524288 | tf_op jit(solution)/shard_map/all_to_all | solution.py:145
  257.0 0.9 copy.73
  257.8 0.0 all-gather.3.cloned.1.call-update
  257.9 0.1 copy.75
  258.0 0.1 copy.78
  258.1 0.1 copy.77
  258.3 0.0 copy-start.19
  258.3 5.9 %fusion.5 = bf16[1,2048,384]{2,1,0:T(8,128)(2,1)} fusion(bf16[1024,384]{1,0:T(8,128)(2,1)S(1)} %get-tuple-element.41, bf16[1,1024,4096]{2,1,0:T(8,128)(2,1)} %bitcast.155), kind=kOutput, calls=%fused_computation.19 | convolution fusion | flops 1611399168 | bytes 6553600 | tf_op jit(solution)/shard_map/dot_general | solution.py:71
  264.2 5.4 %fusion.7 = bf16[1,384,2048]{2,1,0:T(8,128)(2,1)} fusion(bf16[1,1024,4096]{2,1,0:T(8,128)(2,1)} %bitcast.156, f32[1024,384]{1,0:T(8,128)S(1)} %copy-done.19, f32[1024,384]{1,0:T(8,128)S(1)} %copy-done.17), kind=kOutput, calls=%fused_computation.21 | convolution fusion | flops 1613758464 | bytes 8912896 | tf_op jit(solution)/shard_map/dot_general | solution.py:71
  269.6 26.8 %all-gather.3.cloned.1.call-done = bf16[16,16,4,2048]{3,1,2,0:T(8,128)(2,1)} async-done(((bf16[1,16,4,2048]{3,1,2,0:T(8,128)(2,1)}), bf16[16,16,4,2048]{3,1,2,0:T(8,128)(2,1)}) %all-gather.3.cloned.1.call-update) | async-done | bytes 4194320 | tf_op jit(solution)/shard_map/all_gather | solution.py:12
  296.4 6.5 %convert_bitcast_fusion = f32[16,1,16,4,2048]{4,0,3,2,1:T(8,128)} fusion(bf16[16,16,4,2048]{3,1,2,0:T(8,128)(2,1)} %all-gather.3.cloned.1.call-done), kind=kLoop, calls=%fused_computation.5 | loop fusion | flops 2097152 | bytes 12582912 | tf_op jit(solution)/shard_map/convert_element_type | solution.py:148
  302.9 12.0 %copy.74 = f32[16,1,16,4,2048]{4,3,2,0,1:T(4,128)} copy(f32[16,1,16,4,2048]{4,0,3,2,1:T(8,128)} %convert_bitcast_fusion) | data formatting | bytes 16777216 | tf_op jit(solution)/shard_map/convert_element_type | solution.py:148
  314.9 10.0 %reshape.162 = f32[1024,2048]{1,0:T(8,128)} reshape(f32[16,1,16,4,2048]{4,3,2,0,1:T(4,128)} %copy.74) | data formatting | bytes 16777216 | tf_op jit(solution)/shard_map/convert_element_type | solution.py:148
  324.9 9.0 %gather_fusion.2 = f32[512,2048]{1,0:T(8,128)} fusion(f32[1024,2048]{1,0:T(8,128)} %reshape.162, s32[1024]{0:T(1024)S(1)} %pad_clamp_fusion), kind=kCustom, calls=%fused_computation.2 | custom fusion | bytes 8390656 | tf_op jit(solution)/shard_map/gather | solution.py:149
  333.8 5.8 %reshape.160 = f32[256,2,2048]{2,1,0:T(2,128)} reshape(f32[512,2048]{1,0:T(8,128)} %gather_fusion.2) | data formatting | bytes 8388608 | tf_op jit(solution)/shard_map/reshape | solution.py:149
  339.7 8.6 %reduce_sum.58 = f32[256,2048]{1,0:T(8,128)} reduce(f32[256,2,2048]{2,1,0:T(2,128)} %reshape.160, f32[]{:T(128)} %constant.44.clone.1), dimensions={1}, to_apply=%region_5.6 | reduce | flops 524288 | bytes 6291460 | tf_op jit(solution)/shard_map/reduce_sum | solution.py:150
  348.3 2.1 fusion.123
  350.5 0.6 broadcast_in_dim.51
  351.1 4.4 %all-to-all-start.3 = ((f32[16,1,512]{2,1,0:T(1,128)}), f32[16,1,512]{2,1,0:T(1,128)S(1)}, u32[]{:S(2)}, u32[]{:S(2)}) async-start(f32[16,1,512]{2,1,0:T(1,128)} %broadcast_in_dim.51), calls=%async_computation.4 | async-start | bytes 65536 | tf_op jit(solution)/shard_map/all_to_all | solution.py:47
  355.5 3.1 convolution_convert_fusion.2
  358.6 4.6 %all-to-all-done.3 = f32[16,1,512]{2,1,0:T(1,128)S(1)} async-done(((f32[16,1,512]{2,1,0:T(1,128)}), f32[16,1,512]{2,1,0:T(1,128)S(1)}, u32[]{:S(2)}, u32[]{:S(2)}) %all-to-all-start.3) | async-done | bytes 32800 | tf_op jit(solution)/shard_map/all_to_all | solution.py:47
  363.2 7.2 %all-to-all-start.2 = ((bf16[16,128,128]{2,1,0:T(8,128)(2,1)}), bf16[16,128,128]{2,1,0:T(8,128)(2,1)S(1)}, u32[]{:S(2)}, u32[]{:S(2)}) async-start(bf16[16,128,128]{2,1,0:T(8,128)(2,1)} %bitcast.17), calls=%async_computation.3 | async-start | bytes 1048576 | tf_op jit(solution)/shard_map/all_to_all | solution.py:41
  370.5 0.2 subtract_multiply_fusion
  370.7 5.1 %collective-permute-start = (f32[128,30]{0,1:T(8,128)S(1)}, f32[128,30]{0,1:T(8,128)S(1)}, u32[]{:S(2)}, u32[]{:S(2)}) collective-permute-start(f32[128,30]{0,1:T(8,128)S(1)} %slice.271), channel_id=1, source_target_pairs={{16,0},{32,16},{48,32},{64,48},{80,64},{96,80},{112,96},{128,112},... | collective-permute-start | bytes 46088 | tf_op jit(solution)/shard_map/ppermute | solution.py:67
  375.8 5.8 %fusion.6 = bf16[1,2048,384]{2,1,0:T(8,128)(2,1)} fusion(bf16[1024,384]{1,0:T(8,128)(2,1)S(1)} %get-tuple-element.40, bf16[1,1024,4096]{2,1,0:T(8,128)(2,1)} %bitcast.157), kind=kOutput, calls=%fused_computation.20 | convolution fusion | flops 1611399168 | bytes 6553600 | tf_op jit(solution)/shard_map/dot_general | solution.py:71
  381.7 0.4 multiply_convert_fusion.5
  382.1 0.7 copy.79
  382.9 0.7 copy.80
  383.6 0.7 convert_reduce_fusion
  (53 shorter events, 0.3 us)
Async XLA Ops:
  7.2 153.5 %copy-start = (bf16[1,2048,384]{2,1,0:T(8,128)(2,1)S(1)}, bf16[1,2048,384]{2,1,0:T(8,128)(2,1)}, u32[]{:S(2)}) copy-start(bf16[1,2048,384]{2,1,0:T(8,128)(2,1)} %param.19) | copy-start | bytes 4718596
  7.2 235.0 %reduce-scatter.2.cloned.1.call-start = ((), (), s32[]{:S(2)}) async-start(), calls=%async_computation.5 | async-start | bytes 4456448 | tf_op jit(solution)/shard_map/reduce_scatter | solution.py:142
  18.8 6.1 %copy-start.13 = (f32[256,2]{0,1:T(2,128)S(1)}, f32[256,2]{0,1:T(2,128)}, u32[]{:S(2)}) copy-start(f32[256,2]{0,1:T(2,128)} %param.18) | copy-start | bytes 6148
  29.0 10.8 %copy-start.2 = (bf16[256,2048]{1,0:T(8,128)(2,1)S(1)}, bf16[256,2048]{1,0:T(8,128)(2,1)}, u32[]{:S(2)}) copy-start(bf16[256,2048]{1,0:T(8,128)(2,1)} %param.15) | copy-start | bytes 3145732
  160.6 4.9 %copy-start.4 = (bf16[16,64,4096]{2,1,0:T(8,128)(2,1)}, bf16[16,64,4096]{2,1,0:T(8,128)(2,1)S(1)}, u32[]{:S(2)}) copy-start(bf16[16,64,4096]{2,1,0:T(8,128)(2,1)S(1)} %all_to_all.35) | copy-start | bytes 25165828
  160.6 2.6 copy-start.5
  163.2 2.4 copy-start.16
  163.2 2.6 copy-start.15
  165.8 2.8 copy-start.18
  177.6 80.2 %copy-start.7 = (bf16[128,256]{1,0:T(8,128)(2,1)S(1)}, bf16[128,256]{1,0:T(8,128)(2,1)}, u32[]{:S(2)}) copy-start(bf16[128,256]{1,0:T(8,128)(2,1)} %param.27) | copy-start | bytes 196612
  177.6 80.4 %copy-start.8 = (bf16[128,256]{1,0:T(8,128)(2,1)S(1)}, bf16[128,256]{1,0:T(8,128)(2,1)}, u32[]{:S(2)}) copy-start(bf16[128,256]{1,0:T(8,128)(2,1)} %param.25) | copy-start | bytes 196612
  177.6 80.5 %copy-start.9 = (bf16[128,256]{1,0:T(8,128)(2,1)S(1)}, bf16[128,256]{1,0:T(8,128)(2,1)}, u32[]{:S(2)}) copy-start(bf16[128,256]{1,0:T(8,128)(2,1)} %param.26) | copy-start | bytes 196612
  177.6 80.6 %copy-start.10 = (f32[31,128]{1,0:T(8,128)S(1)}, f32[31,128]{1,0:T(8,128)}, u32[]{:S(2)}) copy-start(f32[31,128]{1,0:T(8,128)} %param.24) | copy-start | bytes 47620
  177.7 118.7 %all-gather.3.cloned.1.call-start = ((), (), s32[]{:S(2)}) async-start(), calls=%async_computation.6 | async-start | bytes 4456448 | tf_op jit(solution)/shard_map/all_gather | solution.py:12
  258.3 5.9 %copy-start.17 = (f32[1024,384]{1,0:T(8,128)S(1)}, f32[1024,384]{1,0:T(8,128)}, u32[]{:S(2)}) copy-start(f32[1024,384]{1,0:T(8,128)} %copy-done.16) | copy-start | bytes 4718596
  258.3 5.9 %copy-start.19 = (f32[1024,384]{1,0:T(8,128)S(1)}, f32[1024,384]{1,0:T(8,128)}, u32[]{:S(2)}) copy-start(f32[1024,384]{1,0:T(8,128)} %copy-done.18) | copy-start | bytes 4718596
  339.7 8.7 %copy-start.3 = (bf16[256,2048]{1,0:T(8,128)(2,1)S(1)}, bf16[256,2048]{1,0:T(8,128)(2,1)}, u32[]{:S(2)}) copy-start(bf16[256,2048]{1,0:T(8,128)(2,1)} %param.16) | copy-start | bytes 3145732
  339.7 8.7 %copy-start.6 = (bf16[2048,128]{1,0:T(8,128)(2,1)S(1)}, bf16[2048,128]{1,0:T(8,128)(2,1)}, u32[]{:S(2)}) copy-start(bf16[2048,128]{1,0:T(8,128)(2,1)} %param.22) | copy-start | bytes 1572868
  339.7 8.7 %copy-start.11 = (f32[256]{0:T(256)S(1)}, f32[256]{0:T(256)}, u32[]{:S(2)}) copy-start(f32[256]{0:T(256)} %param.29) | copy-start | bytes 3076
  339.7 8.7 %copy-start.12 = (f32[256]{0:T(256)S(1)}, f32[256]{0:T(256)}, u32[]{:S(2)}) copy-start(f32[256]{0:T(256)} %param.28) | copy-start | bytes 3076
  339.7 8.7 %copy-start.14 = (f32[128]{0:T(128)S(1)}, f32[128]{0:T(128)}, u32[]{:S(2)}) copy-start(f32[128]{0:T(128)} %param.23) | copy-start | bytes 1540
  351.1 12.1 %all-to-all-start.3 = ((f32[16,1,512]{2,1,0:T(1,128)}), f32[16,1,512]{2,1,0:T(1,128)S(1)}, u32[]{:S(2)}, u32[]{:S(2)}) async-start(f32[16,1,512]{2,1,0:T(1,128)} %broadcast_in_dim.51), calls=%async_computation.4 | async-start | bytes 65536 | tf_op jit(solution)/shard_map/all_to_all | solution.py:47
  363.2 20.4 %all-to-all-start.2 = ((bf16[16,128,128]{2,1,0:T(8,128)(2,1)}), bf16[16,128,128]{2,1,0:T(8,128)(2,1)S(1)}, u32[]{:S(2)}, u32[]{:S(2)}) async-start(bf16[16,128,128]{2,1,0:T(8,128)(2,1)} %bitcast.17), calls=%async_computation.3 | async-start | bytes 1048576 | tf_op jit(solution)/shard_map/all_to_all | solution.py:41
  370.7 11.0 %collective-permute-start = (f32[128,30]{0,1:T(8,128)S(1)}, f32[128,30]{0,1:T(8,128)S(1)}, u32[]{:S(2)}, u32[]{:S(2)}) collective-permute-start(f32[128,30]{0,1:T(8,128)S(1)} %slice.271), channel_id=1, source_target_pairs={{16,0},{32,16},{48,32},{64,48},{80,64},{96,80},{112,96},{128,112},... | collective-permute-start | bytes 46088 | tf_op jit(solution)/shard_map/ppermute | solution.py:67
  375.8 8.5 %copy-start.1 = (bf16[1,2048,384]{2,1,0:T(8,128)(2,1)S(1)}, bf16[1,2048,384]{2,1,0:T(8,128)(2,1)}, u32[]{:S(2)}) copy-start(bf16[1,2048,384]{2,1,0:T(8,128)(2,1)} %param.19) | copy-start | bytes 4718596
Sparse Core Ops, SparseCore 0:
  177.8 64.3 reduce-scatter.1
  258.0 38.3 all-gather.2
